TPU v7x, 32 devices: a whole 2x2x4 slice. The times are simulated.
32 devices in a mesh: kv: 16 (over z, y, x), tp: 2 (over core).
Axes of the slice: x: 2, y: 2, z: 4, core: 2. Of those that a mesh axis runs over, the one named last changes fastest.
Arguments:
- hidden_in: bfloat16 [64, 2048], P('tp', 'kv'), may hold values from -20 to 20
- gain_before: float32 [2048], P('kv'), may hold values from 0.1 to 1.9
- gate_before: bfloat16 [2048, 5632], P('kv', 'tp'), may hold values from -0.125 to 0.125
- lift_before: bfloat16 [2048, 5632], P('kv', 'tp'), may hold values from -0.125 to 0.125
- drop_before: bfloat16 [5632, 2048], P('tp', 'kv'), may hold values from -0.078125 to 0.078125
- mixer_gain: float32 [2048], P('kv'), may hold values from 0.1 to 1.9
- value_proj: bfloat16 [2048, 2048], P('kv', 'tp'), may hold values from -0.125 to 0.125
- gate_proj: bfloat16 [2048, 2048], P('kv', 'tp'), may hold values from -0.125 to 0.125
- key_proj: bfloat16 [2048, 1024], P('kv', 'tp'), may hold values from -0.125 to 0.125
- query_proj: bfloat16 [2048, 1024], P('kv', 'tp'), may hold values from -0.125 to 0.125
- step_proj: bfloat16 [2048, 32], P('kv'), may hold values from -0.125 to 0.125
- value_taps: float32 [4, 2048], P(None, 'tp'), may hold values from -3 to 3
- key_taps: float32 [4, 1024], P(None, 'tp'), may hold values from -3 to 3
- query_taps: float32 [4, 1024], P(None, 'tp'), may hold values from -3 to 3
- value_past: bfloat16 [64, 3, 2048], P('kv', None, 'tp'), may hold values from -6 to 6
- key_past: bfloat16 [64, 3, 1024], P('kv', None, 'tp'), may hold values from -6 to 6
- query_past: bfloat16 [64, 3, 1024], P('kv', None, 'tp'), may hold values from -6 to 6
- decay_rate: float32 [32], P('tp'), may hold values from 0.05 to 1
- block_state: float32 [64, 32, 64, 128], P('kv', 'tp'), may hold values from -24 to 24
- block_keys: bfloat16 [64, 128, 1024], P('kv', None, 'tp'), may hold values from -6 to 6
- block_values: bfloat16 [64, 128, 2048], P('kv', None, 'tp'), may hold values from -6 to 6
- block_steps: float32 [64, 128, 32], P('kv', None, 'tp'), may hold values from 0.2 to 2
- block_decay: float32 [64, 128, 32], P('kv', None, 'tp'), may hold values from -1.25 to 0
- lengths: int32 [64], P('kv'), may hold values from 1 to 128, 2048 in all
- head_gain: float32 [2048], P('tp'), may hold values from 0.1 to 1.9
- out_proj: bfloat16 [2048, 2048], P('tp', 'kv'), may hold values from -0.125 to 0.125
- gain_after: float32 [2048], P('kv'), may hold values from 0.1 to 1.9
- gate_after: bfloat16 [2048, 5632], P('kv', 'tp'), may hold values from -0.125 to 0.125
- lift_after: bfloat16 [2048, 5632], P('kv', 'tp'), may hold values from -0.125 to 0.125
- drop_after: bfloat16 [5632, 2048], P('tp', 'kv'), may hold values from -0.078125 to 0.078125
Outputs:
- hidden_out: bfloat16 [64, 2048], P('tp', 'kv')
Inputs may be any that keep to these rules, and one draw needn't show every extreme that they name: `lengths`: some sequence has all 128 positions filled.
All inputs are finite; a program needn't handle non-finite values. No bound on the sum of `lengths` on one device may be relied on, other than what follows from the above.
Results may differ from a plain program's by a relative error of at most 0.014.
Values may be sent and summed in bfloat16 or wider, within the bound.
A program may use at most 64 MiB of HBM per device.

v0:
```python
import jax
import jax.numpy as jnp
from jax import lax
from jax.sharding import PartitionSpec as P

D = 2048
GROUPS = 8
HEADS = 32


EPSILON = 1e-06


def gather_rows(rows_in, gain_vec):
    whole_rows = lax.all_gather(rows_in, "tp", axis=0, tiled=True)
    values = whole_rows.astype(jnp.float32)
    squares = jnp.sum(values * values, axis=1)
    scaled = (values * gain_vec[None, :]).astype(jnp.bfloat16)
    return (scaled, squares)


def inverse_scale(totals):
    return lax.rsqrt(totals / D + EPSILON)[:, None]


def own_rows(totals, row_count):
    return lax.dynamic_slice_in_dim(totals, lax.axis_index("kv") * row_count, row_count, 0)


def finish(partial_value):
    return lax.psum_scatter(
        partial_value.astype(jnp.float32).astype(jnp.bfloat16),
        "tp",
        scatter_dimension=0,
        tiled=True,
    ).astype(jnp.float32)


def half_mlp(rows_in, gain_vec, gate_weight, lift_weight, drop_weight):
    scaled, squares = gather_rows(rows_in, gain_vec)
    totals = lax.psum(squares, "kv")
    gate_part = jnp.dot(scaled, gate_weight, preferred_element_type=jnp.float32)
    lift_part = jnp.dot(scaled, lift_weight, preferred_element_type=jnp.float32)
    gate_sum, lift_sum = lax.psum((gate_part, lift_part), "kv")
    row_scale = inverse_scale(totals)
    hidden = (jax.nn.silu(gate_sum * row_scale) * (lift_sum * row_scale)).astype(jnp.bfloat16)
    partial_value = jnp.dot(hidden, drop_weight, preferred_element_type=jnp.float32).astype(
        jnp.bfloat16
    )
    return finish(partial_value)


def convolve(past_rows, taps, newest):
    earlier = jnp.sum(past_rows.astype(jnp.float32) * taps[None, :-1, :], axis=1)
    return jax.nn.silu(earlier + taps[-1][None, :] * newest)


def mixer(
    rows_in,
    mixer_gain,
    value_proj,
    gate_proj,
    key_proj,
    query_proj,
    step_proj,
    value_taps,
    key_taps,
    query_taps,
    value_past,
    key_past,
    query_past,
    decay_rate,
    block_state,
    block_keys,
    block_values,
    block_steps,
    block_decay,
    lengths,
    head_gain,
    out_proj,
):
    scaled, squares = gather_rows(rows_in, mixer_gain)
    seq_count = lengths.shape[0]
    value_part = jnp.dot(scaled, value_proj, preferred_element_type=jnp.float32)
    gate_part = jnp.dot(scaled, gate_proj, preferred_element_type=jnp.float32)
    key_part = jnp.dot(scaled, key_proj, preferred_element_type=jnp.float32)
    query_part = jnp.dot(scaled, query_proj, preferred_element_type=jnp.float32)
    step_part = jnp.dot(scaled, step_proj, preferred_element_type=jnp.float32)
    totals = own_rows(lax.psum(squares, "kv"), seq_count)
    value_raw, gate_raw, key_raw, query_raw, step_all = (
        lax.psum_scatter(value_part, "kv", scatter_dimension=0, tiled=True),
        lax.psum_scatter(gate_part, "kv", scatter_dimension=0, tiled=True),
        lax.psum_scatter(key_part, "kv", scatter_dimension=0, tiled=True),
        lax.psum_scatter(query_part, "kv", scatter_dimension=0, tiled=True),
        lax.psum_scatter(step_part, "kv", scatter_dimension=0, tiled=True),
    )
    row_scale = inverse_scale(totals)
    heads_here = decay_rate.shape[0]
    step_raw = (
        lax.dynamic_slice_in_dim(step_all, lax.axis_index("tp") * heads_here, heads_here, 1)
        * row_scale
    )
    new_value = convolve(value_past, value_taps, value_raw * row_scale)
    gate_vals = gate_raw * row_scale
    new_key = convolve(key_past, key_taps, key_raw * row_scale)
    new_query = convolve(query_past, query_taps, query_raw * row_scale)
    step_size = jax.nn.softplus(step_raw)
    new_decay = -decay_rate[None, :] * step_size
    block_len = block_keys.shape[1]
    head_dim = block_state.shape[2]
    state_size = block_state.shape[3]
    per_group = HEADS // GROUPS
    group_count = heads_here // per_group
    live_mask = (jnp.arange(block_len, dtype=jnp.int32)[None, :] < (lengths - 1)[:, None])[
        :, :, None
    ]
    masked = jnp.where(live_mask, block_decay, 0.0)
    running = jnp.cumsum(masked, axis=1)
    block_total = running[:, -1, :]
    tail_sum = block_total[:, None, :] - running
    query_round = new_query.astype(jnp.bfloat16).reshape(seq_count, group_count, state_size)
    scores = jnp.einsum(
        "slgn,sgn->slg",
        block_keys.reshape(seq_count, block_len, group_count, state_size),
        query_round,
        preferred_element_type=jnp.float32,
    )
    scores = jnp.repeat(scores, per_group, axis=2)
    weights = jnp.where(
        live_mask, jnp.exp(tail_sum + new_decay[:, None, :]) * block_steps * scores, 0.0
    ).astype(jnp.bfloat16)
    from_block = jnp.einsum(
        "slh,slhp->shp",
        weights,
        block_values.reshape(seq_count, block_len, heads_here, head_dim),
        preferred_element_type=jnp.float32,
    )
    query_heads = jnp.repeat(
        new_query.reshape(seq_count, group_count, state_size), per_group, axis=1
    )
    source_state = jnp.einsum(
        "shpn,shn->shp", block_state, query_heads, precision=lax.Precision.HIGHEST
    )
    source_state = source_state * jnp.exp(block_total + new_decay)[:, :, None]
    self_score = jnp.repeat(
        jnp.sum((new_query * new_key).reshape(seq_count, group_count, state_size), axis=2),
        per_group,
        axis=1,
    )
    from_token = (step_size * self_score)[:, :, None] * new_value.reshape(
        seq_count, heads_here, head_dim
    )
    gated_out = (source_state + from_block + from_token) * jax.nn.silu(
        gate_vals.reshape(seq_count, heads_here, head_dim)
    )
    normed = gated_out * lax.rsqrt(jnp.mean(gated_out * gated_out, axis=2, keepdims=True) + EPSILON)
    normed = normed * head_gain.reshape(heads_here, head_dim)[None]
    mixed_rows = normed.reshape(seq_count, heads_here * head_dim).astype(jnp.bfloat16)
    partial_value = jnp.dot(
        lax.all_gather(mixed_rows, "kv", axis=0, tiled=True),
        out_proj,
        preferred_element_type=jnp.float32,
    ).astype(jnp.bfloat16)
    return finish(partial_value)


def on_device(
    hidden_in,
    gain_before,
    gate_before,
    lift_before,
    drop_before,
    mixer_gain,
    value_proj,
    gate_proj,
    key_proj,
    query_proj,
    step_proj,
    value_taps,
    key_taps,
    query_taps,
    value_past,
    key_past,
    query_past,
    decay_rate,
    block_state,
    block_keys,
    block_values,
    block_steps,
    block_decay,
    lengths,
    head_gain,
    out_proj,
    gain_after,
    gate_after,
    lift_after,
    drop_after,
):
    section_one = (
        hidden_in.astype(jnp.float32)
        + 0.5 * half_mlp(hidden_in, gain_before, gate_before, lift_before, drop_before)
    ).astype(jnp.bfloat16)
    branch_mix = mixer(
        section_one,
        mixer_gain,
        value_proj,
        gate_proj,
        key_proj,
        query_proj,
        step_proj,
        value_taps,
        key_taps,
        query_taps,
        value_past,
        key_past,
        query_past,
        decay_rate,
        block_state,
        block_keys,
        block_values,
        block_steps,
        block_decay,
        lengths,
        head_gain,
        out_proj,
    )
    section_two = (section_one.astype(jnp.float32) + branch_mix).astype(jnp.bfloat16)
    return (
        section_two.astype(jnp.float32)
        + 0.5 * half_mlp(section_two, gain_after, gate_after, lift_after, drop_after)
    ).astype(jnp.bfloat16)


def solution(mesh):
    return jax.shard_map(
        on_device,
        mesh=mesh,
        in_specs=(
            P("tp", "kv"),
            P("kv"),
            P("kv", "tp"),
            P("kv", "tp"),
            P("tp", "kv"),
            P("kv"),
            P("kv", "tp"),
            P("kv", "tp"),
            P("kv", "tp"),
            P("kv", "tp"),
            P("kv", None),
            P(None, "tp"),
            P(None, "tp"),
            P(None, "tp"),
            P("kv", None, "tp"),
            P("kv", None, "tp"),
            P("kv", None, "tp"),
            P("tp"),
            P("kv", "tp", None, None),
            P("kv", None, "tp"),
            P("kv", None, "tp"),
            P("kv", None, "tp"),
            P("kv", None, "tp"),
            P("kv"),
            P("tp"),
            P("tp", "kv"),
            P("kv"),
            P("kv", "tp"),
            P("kv", "tp"),
            P("tp", "kv"),
        ),
        out_specs=P("tp", "kv"),
        check_vma=False,
    )
```

profile of v0, /device:TPU:0, one launch (start us, length us, event | category | flops | bytes accessed | tf_op | source)
XLA Modules:
  0.0 464.0 jit_solution(2448503861973463744)
XLA Ops:
  6.5 2.3 all_gather.12
  8.8 2.2 fusion.13
  11.1 2.2 fusion.15
  13.5 43.7 %psum.50 = f32[64]{0:T(128)S(1)} all-reduce(f32[64]{0:T(128)S(1)} %fusion.2), channel_id=1, replica_groups=mesh['kv'=16,'tp'=2] {'kv'}, use_global_device_ids=true, to_apply=%region_2.0 | all-reduce | flops 64 | bytes 512 | tf_op jit(solution)/shard_map/psum | solution.py:41
  57.2 75.0 %all-reduce.17.cloned.1.call-done = (f32[64,2816]{1,0:T(8,128)}, f32[64,2816]{1,0:T(8,128)}) async-done(((f32[64,2816]{1,0:T(8,128)}, f32[64,2816]{1,0:T(8,128)}), (f32[64,2816]{1,0:T(8,128)}, f32[64,2816]{1,0:T(8,128)})) %all-reduce.17.cloned.1.call-update) | async-done | bytes 1441808 | tf_op jit(solution)/shard_map/psum | solution.py:44
  132.2 2.6 convolution_convert_fusion.1
  135.0 7.0 %reduce-scatter.4.cloned.1.call-done = bf16[32,128]{1,0:T(8,128)(2,1)} async-done(((bf16[64,128]{1,0:T(8,128)(2,1)}), bf16[32,128]{1,0:T(8,128)(2,1)}) %reduce-scatter.4.cloned.1.call-update) | async-done | bytes 8208 | tf_op jit(solution)/shard_map/reduce_scatter | solution.py:31
  142.0 0.7 add_convert_fusion.2
  142.7 1.8 all_gather.13
  144.6 0.9 fusion.22
  145.5 0.9 fusion.24
  146.3 0.8 fusion.26
  147.1 0.8 fusion.30
  148.2 0.3 copy.54
  148.5 0.1 copy.43
  148.6 0.3 reduce_window_sum.11
  148.9 0.6 dynamic-slice
  150.3 2.3 copy.46
  152.8 0.1 fusion.28
  153.0 77.1 %all-reduce.5 = (f32[64]{0:T(128)S(1)}, f32[64,32]{1,0:T(8,128)S(1)}) all-reduce(f32[64]{0:T(128)S(1)} %fusion.4, f32[64,32]{1,0:T(8,128)S(1)} %fusion.28), channel_id=1, replica_groups=mesh['kv'=16,'tp'=2] {'kv'}, use_global_device_ids=true, to_apply=%region_8.9 | all-reduce | flops 2112 | bytes 16896 | tf_op jit(solution)/shard_map/psum | solution.py:89
  230.2 30.9 %all-reduce.15.cloned.1.call-done = (f32[64,1024]{1,0:T(8,128)}, f32[64,1024]{1,0:T(8,128)}, f32[64,512]{1,0:T(8,128)}, f32[64,512]{1,0:T(8,128)}) async-done(((f32[64,1024]{1,0:T(8,128)}, f32[64,1024]{1,0:T(8,128)}, f32[64,512]{1,0:T(8,128)}, f32[64,512]{1,0:T(8,128)}), (f32[64,1024]{1,0:T(8,128)}, f32[64,1024]{1,0:T(8,128)}, f32[64,512]{1,0:T(8,128)}, f32[64,512]{1,0:T(8,128)})) %all-reduce.15.cloned.1.call-update) | async-done | bytes 786448
  261.1 0.8 fusion.17
  262.0 0.2 fusion.36
  262.2 0.1 copy.45
  262.6 0.7 add_exponential_fusion
  263.3 0.1 fusion
  263.6 0.9 divide_multiply_fusion
  264.5 0.7 reshape.84
  265.1 0.7 reshape.85
  265.8 1.9 fusion.37
  267.8 3.4 fusion.35
  271.2 0.9 multiply_reduce_fusion.1
  272.0 0.7 multiply_convert_fusion.4
  272.7 0.8 reshape.86
  273.5 41.6 %all-gather = bf16[16,4,1024]{2,1,0:T(4,128)(2,1)} all-gather(bf16[1,4,1024]{2,1,0:T(4,128)(2,1)S(1)} %reshape.86), channel_id=1, replica_groups=mesh['kv'=16,'tp'=2] {'kv'}, dimensions={0}, use_global_device_ids=true | all-gather | bytes 139264 | tf_op jit(solution)/shard_map/all_gather | solution.py:160
  315.1 1.6 reshape.87
  316.7 1.8 convolution_convert_fusion.2
  318.6 3.5 reduce-scatter.6.cloned.1.call-done
  322.0 0.7 add_convert_fusion.1
  322.7 0.6 copy-done.10
  323.3 1.8 all_gather.15
  325.1 1.8 fusion.11
  326.9 1.8 fusion.9
  328.9 42.2 %psum.54 = f32[64]{0:T(128)S(1)} all-reduce(f32[64]{0:T(128)S(1)} %fusion.6), channel_id=1, replica_groups=mesh['kv'=16,'tp'=2] {'kv'}, use_global_device_ids=true, to_apply=%region_21.22 | all-reduce | flops 64 | bytes 512 | tf_op jit(solution)/shard_map/psum | solution.py:41
  371.1 75.0 %all-reduce.13.cloned.1.call-done = (f32[64,2816]{1,0:T(8,128)}, f32[64,2816]{1,0:T(8,128)}) async-done(((f32[64,2816]{1,0:T(8,128)}, f32[64,2816]{1,0:T(8,128)}), (f32[64,2816]{1,0:T(8,128)}, f32[64,2816]{1,0:T(8,128)})) %all-reduce.13.cloned.1.call-update) | async-done | bytes 1441808 | tf_op jit(solution)/shard_map/psum | solution.py:44
  446.1 2.6 convolution_convert_fusion
  448.7 7.2 %reduce-scatter.8.cloned.1.call-done = bf16[32,128]{1,0:T(8,128)(2,1)} async-done(((bf16[64,128]{1,0:T(8,128)(2,1)}), bf16[32,128]{1,0:T(8,128)(2,1)}) %reduce-scatter.8.cloned.1.call-update) | async-done | bytes 8208 | tf_op jit(solution)/shard_map/reduce_scatter | solution.py:31
  455.8 1.3 add_convert_fusion
  (98 shorter events, 1.7 us)
Async XLA Ops:
  6.5 261.3 %copy-start = (f32[4,16,64,128]{3,2,1,0:T(8,128)S(1)}, f32[4,16,64,128]{3,2,1,0:T(8,128)}, u32[]{:S(2)}) copy-start(f32[4,16,64,128]{3,2,1,0:T(8,128)} %param.48) | copy-start | bytes 6291460
  6.5 125.6 %all-reduce.17.cloned.1.call-start = ((), (), s32[]{:S(2)}) async-start(), calls=%async_computation.8 | async-start | bytes 2883584 | tf_op jit(solution)/shard_map/psum | solution.py:44
  8.8 48.4 %copy-start.26 = (s32[4]{0:T(128)S(1)}, s32[4]{0:T(128)}, u32[]{:S(2)}) copy-start(s32[4]{0:T(128)} %param.53) | copy-start | bytes 52
  13.3 128.7 %reduce-scatter.4.cloned.1.call-start = ((), (), s32[]{:S(2)}) async-start(), calls=%async_computation.3 | async-start | bytes 24576 | tf_op jit(solution)/shard_map/reduce_scatter | solution.py:31
  132.2 9.9 %copy-start.13 = (bf16[32,128]{1,0:T(8,128)(2,1)S(1)}, bf16[32,128]{1,0:T(8,128)(2,1)}, u32[]{:S(2)}) copy-start(bf16[32,128]{1,0:T(8,128)(2,1)} %param.30) | copy-start | bytes 24580
  132.2 12.4 %copy-start.4 = (bf16[128,1024]{1,0:T(8,128)(2,1)S(1)}, bf16[128,1024]{1,0:T(8,128)(2,1)}, u32[]{:S(2)}) copy-start(bf16[128,1024]{1,0:T(8,128)(2,1)} %param.37) | copy-start | bytes 786436
  132.2 12.4 %copy-start.17 = (f32[128]{0:T(128)S(1)}, f32[128]{0:T(128)}, u32[]{:S(2)}) copy-start(f32[128]{0:T(128)} %param.35) | copy-start | bytes 1540
  132.2 13.3 %copy-start.5 = (bf16[128,1024]{1,0:T(8,128)(2,1)S(1)}, bf16[128,1024]{1,0:T(8,128)(2,1)}, u32[]{:S(2)}) copy-start(bf16[128,1024]{1,0:T(8,128)(2,1)} %param.36) | copy-start | bytes 786436
  132.2 14.2 %copy-start.6 = (bf16[128,512]{1,0:T(8,128)(2,1)S(1)}, bf16[128,512]{1,0:T(8,128)(2,1)}, u32[]{:S(2)}) copy-start(bf16[128,512]{1,0:T(8,128)(2,1)} %param.38) | copy-start | bytes 393220
  132.2 14.9 %copy-start.7 = (bf16[128,512]{1,0:T(8,128)(2,1)S(1)}, bf16[128,512]{1,0:T(8,128)(2,1)}, u32[]{:S(2)}) copy-start(bf16[128,512]{1,0:T(8,128)(2,1)} %param.39) | copy-start | bytes 393220
  134.8 13.2 %copy-start.14 = (f32[4,128,16]{1,2,0:T(8,128)S(1)}, f32[4,128,16]{1,2,0:T(8,128)}, u32[]{:S(2)}) copy-start(f32[4,128,16]{1,2,0:T(8,128)} %param.52) | copy-start | bytes 98308
  134.8 13.2 %copy-start.19 = (f32[4,512]{1,0:T(4,128)S(1)}, f32[4,512]{1,0:T(4,128)}, u32[]{:S(2)}) copy-start(f32[4,512]{1,0:T(4,128)} %param.43) | copy-start | bytes 24580
  134.8 13.2 %copy-start.18 = (f32[4,512]{1,0:T(4,128)S(1)}, f32[4,512]{1,0:T(4,128)}, u32[]{:S(2)}) copy-start(f32[4,512]{1,0:T(4,128)} %param.42) | copy-start | bytes 24580
  134.8 13.3 %copy-start.3 = (bf16[4,128,512]{2,1,0:T(8,128)(2,1)S(1)}, bf16[4,128,512]{2,1,0:T(8,128)(2,1)}, u32[]{:S(2)}) copy-start(bf16[4,128,512]{2,1,0:T(8,128)(2,1)} %param.49) | copy-start | bytes 1572868
  134.9 126.2 %all-reduce.15.cloned.1.call-start = ((), (), s32[]{:S(2)}) async-start(), calls=%async_computation.7 | async-start | bytes 1572864
  135.0 13.1 %copy-start.24 = (pred[4,128]{1,0:T(4,128)(4,1)}, pred[4,128]{1,0:T(4,128)(4,1)S(1)}, u32[]{:S(2)}) copy-start(pred[4,128]{1,0:T(4,128)(4,1)S(1)} %iota_compare_fusion) | copy-start | bytes 1540
  144.6 4.3 copy-start.28
  144.6 5.6 %copy-start.27 = (f32[16]{0:T(128)S(1)}, f32[16]{0:T(128)}, u32[]{:S(2)}) copy-start(f32[16]{0:T(128)} %param.47) | copy-start | bytes 196
  144.6 5.6 %copy-start.12 = (f32[4,128,16]{1,2,0:T(8,128)S(1)}, f32[4,128,16]{1,2,0:T(8,128)}, u32[]{:S(2)}) copy-start(f32[4,128,16]{1,2,0:T(8,128)} %param.51) | copy-start | bytes 98308
  148.0 174.1 %reduce-scatter.6.cloned.1.call-start = ((), (), s32[]{:S(2)}) async-start(), calls=%async_computation.4 | async-start | bytes 24576 | tf_op jit(solution)/shard_map/reduce_scatter | solution.py:31
  148.1 4.4 copy-start.15
  148.1 4.4 copy-start.23
  148.1 4.5 copy-start.16
  148.1 4.5 copy-start.20
  148.2 4.5 copy-start.21
  148.2 4.7 %copy-start.22 = (bf16[128,32]{0,1:T(8,128)(2,1)S(1)}, bf16[128,32]{0,1:T(8,128)(2,1)}, u32[]{:S(2)}) copy-start(bf16[128,32]{0,1:T(8,128)(2,1)} %param.40) | copy-start | bytes 24580
  148.6 114.7 %copy-start.25 = (pred[4,128]{1,0:T(4,128)(4,1)S(1)}, pred[4,128]{1,0:T(4,128)(4,1)}, u32[]{:S(2)}) copy-start(pred[4,128]{1,0:T(4,128)(4,1)} %copy-done.24) | copy-start | bytes 1540
  265.8 5.3 %copy-start.8 = (f32[4,16,64]{2,1,0:T(8,128)S(1)}, f32[4,16,64]{2,1,0:T(8,128)}, u32[]{:S(2)}) copy-start(f32[4,16,64]{2,1,0:T(8,128)} %reshape.84) | copy-start | bytes 49156
  265.8 5.3 %copy-start.9 = (f32[4,16,64]{2,1,0:T(8,128)S(1)}, f32[4,16,64]{2,1,0:T(8,128)}, u32[]{:S(2)}) copy-start(f32[4,16,64]{2,1,0:T(8,128)} %reshape.85) | copy-start | bytes 49156
  265.8 59.3 %copy-start.1 = (bf16[128,2816]{1,0:T(8,128)(2,1)S(1)}, bf16[128,2816]{1,0:T(8,128)(2,1)}, u32[]{:S(2)}) copy-start(bf16[128,2816]{1,0:T(8,128)(2,1)} %param.57) | copy-start | bytes 2162692
  267.8 59.1 %copy-start.2 = (bf16[128,2816]{1,0:T(8,128)(2,1)S(1)}, bf16[128,2816]{1,0:T(8,128)(2,1)}, u32[]{:S(2)}) copy-start(bf16[128,2816]{1,0:T(8,128)(2,1)} %param.58) | copy-start | bytes 2162692
  318.5 127.6 %all-reduce.13.cloned.1.call-start = ((), (), s32[]{:S(2)}) async-start(), calls=%async_computation.6 | async-start | bytes 2883584 | tf_op jit(solution)/shard_map/psum | solution.py:44
  322.7 0.6 copy-start.10
  328.7 127.1 %reduce-scatter.8.cloned.1.call-start = ((), (), s32[]{:S(2)}) async-start(), calls=%async_computation.5 | async-start | bytes 24576 | tf_op jit(solution)/shard_map/reduce_scatter | solution.py:31
  446.1 9.8 %copy-start.11 = (bf16[32,128]{1,0:T(8,128)(2,1)S(1)}, bf16[32,128]{1,0:T(8,128)(2,1)}, u32[]{:S(2)}) copy-start(bf16[32,128]{1,0:T(8,128)(2,1)} %copy-done.10) | copy-start | bytes 24580
Sparse Core Ops, SparseCore 0:
  13.5 118.6 all-reduce.16
  135.0 6.9 reduce-scatter.3
  148.1 112.9 all-reduce.14
  318.6 3.3 reduce-scatter.5
  328.8 117.2 all-reduce.12
  448.8 6.9 reduce-scatter.7
where the time goes:
time: 465 us; the launch traced here: 464 us
  blocking collectives  211 us (45%)
  waiting for transfers between devices  199 us (43%)
  matrix products  24 us (5%)
  between operations  14.5 us (3%)
  local copies, waits for them, and re-layouts  8.42 us (2%)
  other arithmetic  7.7 us (2%)
    psum x2, waiting for transfers between devices, half_mlp(): gate_sum, lift_sum = lax.psum((gate_part, lift_part), 'kv')  150 us
    psum x2, blocking collectives, half_mlp(): totals = lax.psum(squares, 'kv')  85.9 us
    psum x1, blocking collectives, mixer(): totals = own_rows(lax.psum(squares, 'kv'), seq_count)  77.1 us
    all_gather x1, blocking collectives, mixer(): lax.all_gather(mixed_rows, 'kv', axis=0, tiled=True)  41.6 us
    unnamed x7, waiting for transfers between devices  31 us
    reduce_scatter x3, waiting for transfers between devices, finish(): lax.psum_scatter(partial_value.astype(jnp.float32).astype(jnp.bfloat16),...  17.7 us
  transfers between devices with their start and end apart: 6, of which 6 were waited for; matrix products, arithmetic and copies ran while one was open for 1% of the time, Pallas kernels for 0%

commit v1 on v0

--- a/solution.py
+++ b/solution.py
@@ -1,7 +1,15 @@
+import functools
+import math
+
 import jax
 import jax.numpy as jnp
 from jax import lax
+from jax.experimental import pallas as pl
+from jax.experimental.pallas import tpu as pltpu
 from jax.sharding import PartitionSpec as P
+
+MESH_ID = pl.DeviceIdType.MESH
+LANES = 128
 
 D = 2048
 GROUPS = 8
@@ -9,6 +17,419 @@
 
 
 EPSILON = 1e-06
+
+
+class Plan:
+    def __init__(self, kv, rows, own_rows, width, hidden, seqs):
+        inner = max(i for i in range(1, math.isqrt(kv) + 1) if kv % i == 0)
+        self.kv, self.inner, self.outer = kv, inner, kv // inner
+        self.rows, self.own_rows, self.width = rows, own_rows, width
+        self.model = width * kv
+        self.group = rows // inner
+        self.seqs = seqs
+        tiles = hidden // LANES
+        wide = -(-tiles // self.outer)
+        self.starts = [c * (tiles - wide) // max(self.outer - 1, 1) * LANES for c in range(self.outer)]
+        self.tiles, self.wide_tiles = tiles, wide
+        self.wide = wide * LANES
+        ends = self.starts[1:] + [tiles * LANES]
+        self.used = [e - s for s, e in zip(self.starts, ends)]
+
+    def start(self, c):
+        first = (c * (self.tiles - self.wide_tiles)) // max(self.outer - 1, 1)
+        return pl.multiple_of(first * LANES, LANES)
+
+
+def place(plan):
+    k = lax.axis_index("kv")
+    return lax.div(k, plan.inner), lax.rem(k, plan.inner), lax.axis_index("tp")
+
+
+def greet(plan, z, p, t):
+    barrier = pltpu.get_barrier_semaphore()
+    for d in range(1, plan.inner):
+        pl.semaphore_signal(barrier, inc=1, device_id=plane_peer(plan, z, p, t, d), device_id_type=MESH_ID)
+    for d in range(1, plan.outer):
+        pl.semaphore_signal(barrier, inc=1, device_id=line_peer(plan, z, p, t, d), device_id_type=MESH_ID)
+    pl.semaphore_signal(barrier, inc=1, device_id=(z * plan.inner + p, 1 - t), device_id_type=MESH_ID)
+    pl.semaphore_wait(barrier, plan.inner + plan.outer - 1)
+
+
+def plane_peer(plan, z, p, t, d):
+    return (z * plan.inner + lax.rem(p + d, plan.inner), t)
+
+
+def line_peer(plan, z, p, t, d):
+    return (lax.rem(z + d, plan.outer) * plan.inner + p, t)
+
+
+def remote(src, dst, sems, index, device):
+    return pltpu.make_async_remote_copy(
+        src_ref=src,
+        dst_ref=dst,
+        send_sem=sems.at[(0,) + index],
+        recv_sem=sems.at[(1,) + index],
+        device_id=device,
+        device_id_type=MESH_ID,
+    )
+
+
+def silu(a):
+    return a / (1.0 + jnp.exp(-a))
+
+
+def unit_scratch(plan):
+    span = 2 * plan.wide + LANES
+    i, o, g = plan.inner, plan.outer, plan.group
+    return [
+        pltpu.VMEM((i, o, g, span), jnp.bfloat16),
+        pltpu.VMEM((i, o, g, span), jnp.bfloat16),
+        pltpu.VMEM((o, g, span), jnp.bfloat16),
+        pltpu.VMEM((o, g, span), jnp.bfloat16),
+        pltpu.VMEM((o, i, g, plan.wide), jnp.bfloat16),
+        pltpu.SemaphoreType.DMA((2, i, o)),
+        pltpu.SemaphoreType.DMA((2, o)),
+        pltpu.SemaphoreType.DMA((2, o)),
+        pltpu.SemaphoreType.DMA((2, i, o)),
+    ]
+
+
+def unit_product(plan, x, gain, gate_ref, lift_ref, drop_ref, scratch):
+    out_buf, in_buf, line_out, line_in, hid, plane_sem, line_sem, hz_sem, hp_sem = scratch
+    z, p, t = place(plan)
+    inner, outer, group, wide = plan.inner, plan.outer, plan.group, plan.wide
+    values = x.astype(jnp.float32)
+    squares = jnp.sum(values * values, axis=1, keepdims=True)
+    squares = jnp.broadcast_to(squares, (plan.rows, LANES)).astype(jnp.bfloat16)
+    scaled = (values * gain).astype(jnp.bfloat16)
+    sends = []
+    plane = []
+    for n in range(outer):
+        c = lax.rem(z + 1 + n, outer)
+        columns = pl.ds(plan.start(c), wide)
+        gate = jnp.dot(scaled, gate_ref[:, columns], preferred_element_type=jnp.float32).astype(jnp.bfloat16)
+        lift = jnp.dot(scaled, lift_ref[:, columns], preferred_element_type=jnp.float32).astype(jnp.bfloat16)
+        for q in range(inner):
+            rows = slice(q * group, (q + 1) * group)
+            out_buf[q, n, :, 0:wide] = gate[rows]
+            out_buf[q, n, :, wide : 2 * wide] = lift[rows]
+            out_buf[q, n, :, 2 * wide :] = squares[rows]
+        copies = []
+        for d in range(1, inner):
+            copy = remote(
+                out_buf.at[lax.rem(p + d, inner), n],
+                in_buf.at[d, n],
+                plane_sem,
+                (d, n),
+                plane_peer(plan, z, p, t, d),
+            )
+            copy.start()
+            copies.append(copy)
+        plane.append(copies)
+        sends.extend(copies)
+    line = []
+    for n in range(outer):
+        total = out_buf[p, n].astype(jnp.float32)
+        for d in range(1, inner):
+            plane[n][d - 1].wait_recv()
+            total = total + in_buf[d, n].astype(jnp.float32)
+        if n < outer - 1:
+            line_out[n] = total.astype(jnp.bfloat16)
+            copy = remote(line_out.at[n], line_in.at[n], line_sem, (n,), line_peer(plan, z, p, t, n + 1))
+            copy.start()
+            line.append(copy)
+    sends.extend(line)
+    for n in range(outer - 1):
+        line[n].wait_recv()
+        total = total + line_in[n].astype(jnp.float32)
+    scale = lax.rsqrt(total[:, 2 * wide :] / plan.model + EPSILON)[:, 0:1]
+    hidden = silu(total[:, 0:wide] * scale) * (total[:, wide : 2 * wide] * scale)
+    hid[z, p] = hidden.astype(jnp.bfloat16)
+    line = []
+    for d in range(1, outer):
+        copy = remote(hid.at[z, p], hid.at[z, p], hz_sem, (d,), line_peer(plan, z, p, t, d))
+        copy.start()
+        line.append(copy)
+    sends.extend(line)
+
+    def from_line(d):
+        source = lax.rem(z + outer - d, outer)
+        return remote(hid.at[source, p], hid.at[source, p], hz_sem, (d,), line_peer(plan, z, p, t, d))
+
+    for n in range(outer):
+        source = lax.rem(z + outer - n, outer)
+        if n > 0:
+            from_line(n).wait_recv()
+        for d in range(1, inner):
+            copy = remote(hid.at[source, p], hid.at[source, p], hp_sem, (d, n), plane_peer(plan, z, p, t, d))
+            copy.start()
+            sends.append(copy)
+    for n in range(outer):
+        source = lax.rem(z + outer - n, outer)
+        for d in range(1, inner):
+            sender = lax.rem(p + inner - d, inner)
+            remote(
+                hid.at[source, sender], hid.at[source, sender], hp_sem, (d, n), plane_peer(plan, z, p, t, d)
+            ).wait_recv()
+    total = jnp.zeros((plan.rows, plan.width), jnp.float32)
+    for c in range(outer):
+        first, used = plan.starts[c], plan.used[c]
+        lhs = hid[c, :, :, 0:used].reshape(plan.rows, used)
+        total = total + jnp.dot(lhs, drop_ref[first : first + used, :], preferred_element_type=jnp.float32)
+    return total.astype(jnp.bfloat16), sends
+
+
+def swap_whole(plan, mine, pair, sem):
+    z, p, t = place(plan)
+    pair[0] = mine
+    copy = remote(pair.at[0], pair.at[1], sem, (0,), (z * plan.inner + p, 1 - t))
+    copy.start()
+    copy.wait()
+    return mine.astype(jnp.float32) + pair[1].astype(jnp.float32)
+
+
+def first_kernel(
+    plan,
+    x_ref,
+    gain_ref,
+    gate_ref,
+    lift_ref,
+    drop_ref,
+    mix_gain_ref,
+    value_ref,
+    mgate_ref,
+    key_ref,
+    query_ref,
+    step_ref,
+    section_ref,
+    raw_ref,
+    gathered,
+    gather_sem,
+    pair,
+    pair_sem,
+    mix_out,
+    mix_in,
+    mline_out,
+    mline_in,
+    mplane_sem,
+    mline_sem,
+    *scratch,
+):
+    z, p, t = place(plan)
+    inner, outer, group, seqs = plan.inner, plan.outer, plan.group, plan.seqs
+    greet(plan, z, p, t)
+    copy = remote(x_ref, gathered.at[t], gather_sem, (0,), (z * inner + p, 1 - t))
+    copy.start()
+    gathered[t] = x_ref[...]
+    remote(x_ref, gathered.at[1 - t], gather_sem, (0,), (z * inner + p, 1 - t)).wait_recv()
+    x = gathered[...].reshape(plan.rows, plan.width)
+    product, sends = unit_product(plan, x, gain_ref[...], gate_ref, lift_ref, drop_ref, scratch)
+    sends.append(copy)
+    unit = swap_whole(plan, product, pair, pair_sem)
+    section = (x.astype(jnp.float32) + 0.5 * unit).astype(jnp.bfloat16)
+    section_ref[...] = section
+    at = lax.broadcasted_iota(jnp.int32, (plan.rows, plan.rows), 0)
+    of = lax.broadcasted_iota(jnp.int32, (plan.rows, plan.rows), 1)
+    own_inner = lax.div(at, outer * seqs)
+    rest = at - own_inner * (outer * seqs)
+    own_outer = lax.div(rest, seqs)
+    wanted = (own_outer * inner + own_inner) * seqs + (rest - own_outer * seqs)
+    moving = jnp.where(of == wanted, 1.0, 0.0).astype(jnp.bfloat16)
+    values = jnp.dot(moving, section, preferred_element_type=jnp.float32)
+    squares = jnp.sum(values * values, axis=1, keepdims=True)
+    scaled = (values * mix_gain_ref[...]).astype(jnp.bfloat16)
+    steps = step_ref.shape[1]
+    row = lax.broadcasted_iota(jnp.int32, (steps, LANES), 0)
+    lane = lax.broadcasted_iota(jnp.int32, (steps, LANES), 1)
+    spread = jnp.where(row == lane, 1.0, 0.0).astype(jnp.bfloat16)
+    step_wide = jnp.dot(step_ref[...], spread, preferred_element_type=jnp.float32).astype(jnp.bfloat16)
+    lanes = lax.broadcasted_iota(jnp.int32, (plan.rows, LANES), 1)
+    last = jnp.dot(scaled, step_wide, preferred_element_type=jnp.float32)
+    last = jnp.where(lanes == LANES - 1, squares, last).astype(jnp.bfloat16)
+    chunks, first = [], 0
+    plane = []
+    for n, refs in enumerate(((key_ref, query_ref), (value_ref,), (mgate_ref,))):
+        low = first
+        pieces = [jnp.dot(scaled, ref[...], preferred_element_type=jnp.float32).astype(jnp.bfloat16) for ref in refs]
+        if n == 0:
+            pieces.append(last)
+        for piece in pieces:
+            size = piece.shape[1]
+            for q in range(inner):
+                mix_out[q, :, first : first + size] = piece[q * group : (q + 1) * group]
+            first = first + size
+        columns = slice(low, first)
+        chunks.append(columns)
+        copies = []
+        for d in range(1, inner):
+            copy = remote(
+                mix_out.at[lax.rem(p + d, inner), :, columns],
+                mix_in.at[d, :, columns],
+                mplane_sem,
+                (d, n),
+                plane_peer(plan, z, p, t, d),
+            )
+            copy.start()
+            copies.append(copy)
+        plane.append(copies)
+        sends.extend(copies)
+    line = []
+    for n, columns in enumerate(chunks):
+        total = mix_out[p, :, columns].astype(jnp.float32)
+        for d in range(1, inner):
+            plane[n][d - 1].wait_recv()
+            total = total + mix_in[d, :, columns].astype(jnp.float32)
+        for o in range(outer):
+            mline_out[o, :, columns] = total[o * seqs : (o + 1) * seqs]
+        copies = []
+        for d in range(1, outer):
+            copy = remote(
+                mline_out.at[lax.rem(z + d, outer), :, columns],
+                mline_in.at[d, :, columns],
+                mline_sem,
+                (d, n),
+                line_peer(plan, z, p, t, d),
+            )
+            copy.start()
+            copies.append(copy)
+        line.append(copies)
+        sends.extend(copies)
+    scale = None
+    for n, columns in enumerate(chunks):
+        total = mline_out[z, :, columns]
+        for d in range(1, outer):
+            line[n][d - 1].wait_recv()
+            total = total + mline_in[d, :, columns]
+        if n == 0:
+            scale = lax.rsqrt(total[:, -1:] / plan.model + EPSILON)
+        raw_ref[:, columns] = total * scale
+    for copy in sends:
+        copy.wait_send()
+
+
+def last_kernel(
+    plan,
+    section_ref,
+    mixed_ref,
+    out_proj_ref,
+    gain_ref,
+    gate_ref,
+    lift_ref,
+    drop_ref,
+    out_ref,
+    mixed,
+    stacked,
+    pair,
+    final_in,
+    final_out,
+    section_buf,
+    mz_sem,
+    mp_sem,
+    pair_sem,
+    final_sem,
+    *scratch,
+):
+    z, p, t = place(plan)
+    inner, outer, seqs = plan.inner, plan.outer, plan.seqs
+    greet(plan, z, p, t)
+    sends = []
+    for d in range(1, outer):
+        copy = remote(mixed_ref, mixed.at[z, p], mz_sem, (d,), line_peer(plan, z, p, t, d))
+        copy.start()
+        sends.append(copy)
+    for n in range(outer):
+        source = lax.rem(z + outer - n, outer)
+        block = mixed_ref if n == 0 else mixed.at[source, p]
+        if n > 0:
+            remote(block, mixed.at[source, p], mz_sem, (n,), line_peer(plan, z, p, t, n)).wait_recv()
+        for d in range(1, inner):
+            copy = remote(block, mixed.at[source, p], mp_sem, (d, n), plane_peer(plan, z, p, t, d))
+            copy.start()
+            sends.append(copy)
+    mixed[z, p] = mixed_ref[...]
+    for n in range(outer):
+        source = lax.rem(z + outer - n, outer)
+        for d in range(1, inner):
+            sender = lax.rem(p + inner - d, inner)
+            remote(
+                mixed_ref, mixed.at[source, sender], mp_sem, (d, n), plane_peer(plan, z, p, t, d)
+            ).wait_recv()
+    for o in range(outer):
+        for i in range(inner):
+            first = (o * inner + i) * seqs
+            stacked[first : first + seqs, :] = mixed[o, i]
+    product = jnp.dot(
+        stacked[...].astype(jnp.bfloat16), out_proj_ref[...], preferred_element_type=jnp.float32
+    ).astype(jnp.bfloat16)
+    branch = swap_whole(plan, product, pair, pair_sem)
+    x = (section_ref[...].astype(jnp.float32) + branch).astype(jnp.bfloat16)
+    section_buf[...] = x.reshape(section_buf.shape)
+    product, more = unit_product(plan, x, gain_ref[...], gate_ref, lift_ref, drop_ref, scratch)
+    final_out[...] = product.reshape(final_out.shape)
+    copy = remote(final_out.at[1 - t], final_in, final_sem, (0,), (z * inner + p, 1 - t))
+    copy.start()
+    copy.wait()
+    unit = final_out[t].astype(jnp.float32) + final_in[...].astype(jnp.float32)
+    out_ref[...] = (section_buf[t].astype(jnp.float32) + 0.5 * unit).astype(jnp.bfloat16)
+    for copy in sends + more:
+        copy.wait_send()
+
+
+def run_first(plan, x, gain, gate, lift, drop, mix_gain, value, mgate, key, query, step):
+    span = value.shape[1] + mgate.shape[1] + key.shape[1] + query.shape[1] + LANES
+    i, o, g, s = plan.inner, plan.outer, plan.group, plan.seqs
+    vmem = pl.BlockSpec(memory_space=pltpu.VMEM)
+    return pl.pallas_call(
+        functools.partial(first_kernel, plan),
+        out_shape=(
+            jax.ShapeDtypeStruct((plan.rows, plan.width), jnp.bfloat16),
+            jax.ShapeDtypeStruct((s, span), jnp.float32),
+        ),
+        in_specs=[vmem] * 11,
+        out_specs=(vmem, vmem),
+        scratch_shapes=[
+            pltpu.VMEM((2, plan.own_rows, plan.width), jnp.bfloat16),
+            pltpu.SemaphoreType.DMA((2, 1)),
+            pltpu.VMEM((2, plan.rows, plan.width), jnp.bfloat16),
+            pltpu.SemaphoreType.DMA((2, 1)),
+            pltpu.VMEM((i, g, span), jnp.bfloat16),
+            pltpu.VMEM((i, g, span), jnp.bfloat16),
+            pltpu.VMEM((o, s, span), jnp.float32),
+            pltpu.VMEM((o, s, span), jnp.float32),
+            pltpu.SemaphoreType.DMA((2, i, 3)),
+            pltpu.SemaphoreType.DMA((2, o, 3)),
+        ]
+        + unit_scratch(plan),
+        compiler_params=pltpu.CompilerParams(collective_id=0, has_side_effects=True),
+        name="unit_and_projections",
+    )(x, gain[None], gate, lift, drop, mix_gain[None], value, mgate, key, query, step)
+
+
+def run_last(plan, section, mixed_rows, out_proj, gain, gate, lift, drop):
+    i, o, s = plan.inner, plan.outer, plan.seqs
+    vmem = pl.BlockSpec(memory_space=pltpu.VMEM)
+    inner_width = out_proj.shape[0]
+    return pl.pallas_call(
+        functools.partial(last_kernel, plan),
+        out_shape=jax.ShapeDtypeStruct((plan.own_rows, plan.width), jnp.bfloat16),
+        in_specs=[vmem] * 7,
+        out_specs=vmem,
+        scratch_shapes=[
+            pltpu.VMEM((o, i, s, inner_width), jnp.float32),
+            pltpu.VMEM((plan.rows, inner_width), jnp.float32),
+            pltpu.VMEM((2, plan.rows, plan.width), jnp.bfloat16),
+            pltpu.VMEM((plan.own_rows, plan.width), jnp.bfloat16),
+            pltpu.VMEM((2, plan.own_rows, plan.width), jnp.bfloat16),
+            pltpu.VMEM((2, plan.own_rows, plan.width), jnp.bfloat16),
+            pltpu.SemaphoreType.DMA((2, o)),
+            pltpu.SemaphoreType.DMA((2, i, o)),
+            pltpu.SemaphoreType.DMA((2, 1)),
+            pltpu.SemaphoreType.DMA((2, 1)),
+        ]
+        + unit_scratch(plan),
+        compiler_params=pltpu.CompilerParams(collective_id=1, has_side_effects=True),
+        name="mix_out_and_unit",
+    )(section, mixed_rows, out_proj, gain[None], gate, lift, drop)
 
 
 def gather_rows(rows_in, gain_vec):
@@ -231,9 +652,240 @@
     ).astype(jnp.bfloat16)
 
 
+def mix_block(
+    value_raw,
+    gate_raw,
+    key_raw,
+    query_raw,
+    step_raw,
+    value_taps,
+    key_taps,
+    query_taps,
+    value_past,
+    key_past,
+    query_past,
+    decay_rate,
+    block_state,
+    block_keys,
+    block_values,
+    block_steps,
+    block_decay,
+    lengths,
+    head_gain,
+):
+    seq_count = lengths.shape[0]
+    heads_here = decay_rate.shape[0]
+    new_value = convolve(value_past, value_taps, value_raw)
+    gate_vals = gate_raw
+    new_key = convolve(key_past, key_taps, key_raw)
+    new_query = convolve(query_past, query_taps, query_raw)
+    step_size = jax.nn.softplus(step_raw)
+    new_decay = -decay_rate[None, :] * step_size
+    block_len = block_keys.shape[1]
+    head_dim = block_state.shape[2]
+    state_size = block_state.shape[3]
+    per_group = HEADS // GROUPS
+    group_count = heads_here // per_group
+    live_mask = (jnp.arange(block_len, dtype=jnp.int32)[None, :] < (lengths - 1)[:, None])[
+        :, :, None
+    ]
+    masked = jnp.where(live_mask, block_decay, 0.0)
+    running = jnp.cumsum(masked, axis=1)
+    block_total = running[:, -1, :]
+    tail_sum = block_total[:, None, :] - running
+    query_round = new_query.astype(jnp.bfloat16).reshape(seq_count, group_count, state_size)
+    scores = jnp.einsum(
+        "slgn,sgn->slg",
+        block_keys.reshape(seq_count, block_len, group_count, state_size),
+        query_round,
+        preferred_element_type=jnp.float32,
+    )
+    scores = jnp.repeat(scores, per_group, axis=2)
+    weights = jnp.where(
+        live_mask, jnp.exp(tail_sum + new_decay[:, None, :]) * block_steps * scores, 0.0
+    ).astype(jnp.bfloat16)
+    from_block = jnp.einsum(
+        "slh,slhp->shp",
+        weights,
+        block_values.reshape(seq_count, block_len, heads_here, head_dim),
+        preferred_element_type=jnp.float32,
+    )
+    query_heads = jnp.repeat(
+        new_query.reshape(seq_count, group_count, state_size), per_group, axis=1
+    )
+    source_state = jnp.einsum(
+        "shpn,shn->shp", block_state, query_heads, precision=lax.Precision.HIGHEST
+    )
+    source_state = source_state * jnp.exp(block_total + new_decay)[:, :, None]
+    self_score = jnp.repeat(
+        jnp.sum((new_query * new_key).reshape(seq_count, group_count, state_size), axis=2),
+        per_group,
+        axis=1,
+    )
+    from_token = (step_size * self_score)[:, :, None] * new_value.reshape(
+        seq_count, heads_here, head_dim
+    )
+    gated_out = (source_state + from_block + from_token) * jax.nn.silu(
+        gate_vals.reshape(seq_count, heads_here, head_dim)
+    )
+    normed = gated_out * lax.rsqrt(jnp.mean(gated_out * gated_out, axis=2, keepdims=True) + EPSILON)
+    normed = normed * head_gain.reshape(heads_here, head_dim)[None]
+    return normed.reshape(seq_count, heads_here * head_dim).astype(jnp.bfloat16)
+
+
+def on_device_fast(
+    hidden_in,
+    gain_before,
+    gate_before,
+    lift_before,
+    drop_before,
+    mixer_gain,
+    value_proj,
+    gate_proj,
+    key_proj,
+    query_proj,
+    step_proj,
+    value_taps,
+    key_taps,
+    query_taps,
+    value_past,
+    key_past,
+    query_past,
+    decay_rate,
+    block_state,
+    block_keys,
+    block_values,
+    block_steps,
+    block_decay,
+    lengths,
+    head_gain,
+    out_proj,
+    gain_after,
+    gate_after,
+    lift_after,
+    drop_after,
+):
+    kv, tp = lax.axis_size("kv"), lax.axis_size("tp")
+    own_rows, width = hidden_in.shape
+    rows, hidden, seqs = own_rows * tp, gate_before.shape[1], lengths.shape[0]
+    plan = Plan(kv, rows, own_rows, width, hidden, seqs)
+    section, raw = run_first(
+        plan,
+        hidden_in,
+        gain_before,
+        gate_before,
+        lift_before,
+        drop_before,
+        mixer_gain,
+        value_proj,
+        gate_proj,
+        key_proj,
+        query_proj,
+        step_proj,
+    )
+    sizes = (key_proj.shape[1], query_proj.shape[1], LANES, value_proj.shape[1], gate_proj.shape[1])
+    ends = [sum(sizes[: n + 1]) for n in range(len(sizes))]
+    key_raw, query_raw, step_all, value_raw, gate_raw = (
+        raw[:, end - size : end] for size, end in zip(sizes, ends)
+    )
+    heads_here = decay_rate.shape[0]
+    step_raw = lax.dynamic_slice_in_dim(step_all, lax.axis_index("tp") * heads_here, heads_here, 1)
+    mixed_rows = mix_block(
+        value_raw,
+        gate_raw,
+        key_raw,
+        query_raw,
+        step_raw,
+        value_taps,
+        key_taps,
+        query_taps,
+        value_past,
+        key_past,
+        query_past,
+        decay_rate,
+        block_state,
+        block_keys,
+        block_values,
+        block_steps,
+        block_decay,
+        lengths,
+        head_gain,
+    )
+    return run_last(
+        plan,
+        section,
+        mixed_rows.astype(jnp.float32),
+        out_proj,
+        gain_after,
+        gate_after,
+        lift_after,
+        drop_after,
+    )
+
+
+def fits(
+    hidden_in,
+    gain_before,
+    gate_before,
+    lift_before,
+    drop_before,
+    mixer_gain,
+    value_proj,
+    gate_proj,
+    key_proj,
+    query_proj,
+    step_proj,
+    value_taps,
+    key_taps,
+    query_taps,
+    value_past,
+    key_past,
+    query_past,
+    decay_rate,
+    block_state,
+    block_keys,
+    block_values,
+    block_steps,
+    block_decay,
+    lengths,
+    head_gain,
+    out_proj,
+    gain_after,
+    gate_after,
+    lift_after,
+    drop_after,
+):
+    kv, tp = lax.axis_size("kv"), lax.axis_size("tp")
+    own_rows, width = hidden_in.shape
+    inner = max(i for i in range(1, math.isqrt(kv) + 1) if kv % i == 0)
+    aligned = (
+        gate_before.shape[1],
+        width,
+        value_proj.shape[1],
+        gate_proj.shape[1],
+        key_proj.shape[1],
+        query_proj.shape[1],
+    )
+    return (
+        tp == 2
+        and inner > 1
+        and all(size % LANES == 0 for size in aligned)
+        and own_rows % 16 == 0
+        and own_rows * tp % (16 * inner) == 0
+        and lengths.shape[0] in (4, 8)
+        and lengths.shape[0] * kv == own_rows * tp
+        and step_proj.shape[1] < LANES
+        and gate_before.shape[1] // LANES >= 2 * (kv // inner)
+    )
+
+
+def choose(*args):
+    return on_device_fast(*args) if fits(*args) else on_device(*args)
+
+
 def solution(mesh):
     return jax.shard_map(
-        on_device,
+        choose,
         mesh=mesh,
         in_specs=(
             P("tp", "kv"),

time: 465 us -> 95.2 us (0.20)
  blocking collectives: 211 us -> 0 us
  waiting for transfers between devices: 199 us -> 0 us
  Pallas kernels: 0 us -> 81.4 us
  matrix products: 24 us -> 4.25 us
  between operations: 14.5 us -> 0.3 us
  other arithmetic: 7.7 us -> 1.76 us
    psum x3 -> x0, blocking collectives: 163 us -> none  [the longest x2 85.9 us: half_mlp(): totals = lax.psum(squares, 'kv')]
    psum x2 -> x0, waiting for transfers between devices: 150 us -> none  [half_mlp(): gate_sum, lift_sum = lax.psum((gate_part, lift_part), 'kv')]
    pallas_call x0 -> x2, Pallas kernels: none -> 81.4 us  [the longest x1 43 us: run_first(): pl.pallas_call(functools.partial(first_kernel, plan), out_shape=(jax.Shap...]
    all_gather x4 -> x0, blocking collectives: 47.5 us -> none  [the longest x1 41.6 us: mixer(): lax.all_gather(mixed_rows, 'kv', axis=0, tiled=True)]
    unnamed x7 -> x0, waiting for transfers between devices: 31 us -> none
    dot_general x15 -> x3, matrix products: 24 us -> 4.25 us  [the longest x1 3.35 us: mix_block(): jnp.einsum('shpn,shn->shp', block_state, query_heads, precision=lax.Preci...]
    reduce_scatter x3 -> x0, waiting for transfers between devices: 17.7 us -> none  [finish(): lax.psum_scatter(partial_value.astype(jnp.float32).astype(jnp.bfloat16),...]
  transfers between devices with their start and end apart: 6 -> 0, of which waited for: 6 -> 0; matrix products, arithmetic and copies ran while one was open for 1% -> 0% of each run, Pallas kernels for 0% -> 0%
where the time goes in v1:
time: 95.2 us; the launch traced here: 94.8 us
  Pallas kernels  81.4 us (86%)
  local copies, waits for them, and re-layouts  7.14 us (8%)
  matrix products  4.25 us (4%)
  other arithmetic  1.76 us (2%)
    pallas_call x1, Pallas kernels, run_first(): pl.pallas_call(functools.partial(first_kernel, plan), out_shape=(jax.Shap...  43 us
    pallas_call x1, Pallas kernels, run_last(): pl.pallas_call(functools.partial(last_kernel, plan), out_shape=jax.ShapeD...  38.4 us
    unnamed x32, local copies, waits for them, and re-layouts  4.66 us
    dot_general x1, matrix products, mix_block(): jnp.einsum('shpn,shn->shp', block_state, query_heads, precision=lax.Preci...  3.35 us

profile of v1, /device:TPU:0, one launch (start us, length us, event | category | flops | bytes accessed | tf_op | source)
XLA Modules:
  0.0 94.8 jit_solution(15124629059573562613)
XLA Ops:
  0.0 0.0 copy-start
  0.0 0.0 copy-start.10
  0.0 0.0 copy-start.12
  0.0 0.0 copy-start.4
  0.0 0.0 copy-start.13
  0.1 0.0 copy-start.1
  0.1 1.6 %copy.36.step_ref = bf16[128,32]{1,0:T(8,128)(2,1)} copy(bf16[128,32]{0,1:T(8,128)(2,1)} %param.40) | data formatting | bytes 16384 | tf_op args[10]
  1.6 43.0 %unit_and_projections.1 = (bf16[64,128]{1,0:T(8,128)(2,1)}, f32[4,3200]{1,0:T(4,128)}) custom-call(bf16[32,128]{1,0:T(8,128)(2,1)} %x_ref.1, f32[1,128]{1,0:T(1,128)} %bitcast.49, bf16[128,2816]{1,0:T(8,128)(2,1)} %gate_ref.2, bf16[128,2816]{1,0:T(8,128)(2,1)} %lift_ref.2, bf16[2816,128]{1,0:T(8,128)(2,1)} %drop_ref.2, f32[1,128]{1,0:T(1,128)} %bitcast.50, ...), custom_call_target="tpu_custom_call" | custom-call | tf_op jit(solution)/shard_map/unit_and_projections/pallas_call | solution.py:382
  44.7 0.0 copy-start.3
  44.7 0.0 copy-done.7
  44.7 0.0 copy-done.8
  44.7 0.0 copy-done.9
  44.7 0.0 copy-done.10
  44.8 0.7 fusion.2
  45.5 0.1 reduce_sum.47
  45.6 0.1 broadcast_in_dim.51
  45.7 0.1 reshape.79
  45.8 0.0 copy-done.12
  45.8 0.1 iota_compare_fusion
  45.9 0.0 copy-done.4
  45.9 0.1 copy.39
  46.0 0.3 reduce_window_sum.11
  46.3 0.7 slice.40
  46.9 0.1 add_exponential_fusion
  47.1 0.0 copy-done.1
  47.1 0.3 copy.50
  47.3 0.3 fusion.5
  47.6 0.1 copy.41
  47.7 0.0 copy-done.3
  47.7 0.1 copy.40
  47.9 0.1 fusion
  48.0 0.1 copy.48
  48.1 1.6 %copy.42 = bf16[4,128,1024]{1,2,0:T(8,128)(2,1)S(1)} copy(bf16[4,128,1024]{2,1,0:T(8,128)(2,1)} %param.50) | data formatting | bytes 2097152 | tf_op args[20]
  49.8 0.0 copy-start.5
  49.8 0.0 copy-start.6
  49.8 0.0 copy-start.2
  49.8 0.0 copy-start.11
  49.8 0.6 fusion.6
  50.5 3.4 %fusion.4 = f32[4,16,1,64]{3,2,1,0:T(1,128)S(1)} fusion(f32[4,16,128,1]{2,3,1,0:T(1,128)S(1)} %bitcast.36, f32[4,16,64,128]{3,2,1,0:T(8,128)S(1)} %copy-done), kind=kOutput, calls=%fused_computation.21 | convolution fusion | flops 6291456 | bytes 2146304 | tf_op jit(solution)/shard_map/shpn,shn->shp/dot_general | solution.py:716
  53.9 0.0 copy-done.5
  54.0 0.1 reshape.80
  54.0 0.1 reshape.81
  54.1 0.2 multiply_reduce_fusion.1
  54.3 0.1 mul.166
  54.4 0.1 fusion.1
  54.5 0.7 reshape.82.mixed_ref
  55.2 38.4 %mix_out_and_unit.1 = bf16[32,128]{1,0:T(8,128)(2,1)} custom-call(bf16[64,128]{1,0:T(8,128)(2,1)} %get-tuple-element.7.section_ref, f32[4,1024]{1,0:T(4,128)} %reshape.82.mixed_ref, bf16[1024,128]{1,0:T(8,128)(2,1)} %out_proj_ref.1, f32[1,128]{1,0:T(1,128)} %bitcast.51, bf16[128,2816]{1,0:T(8,128)(2,1)} %gate_ref.3, bf16[128,2816]{1,0:T(8,128)(2,1)} %lift_ref.3, ...), custom_call_target="tpu_custom_call" | custom-call | tf_op jit(solution)/shard_map/mix_out_and_unit/pallas_call | solution.py:412
  93.5 1.3 %copy.59 = bf16[32,128]{1,0:T(8,128)(2,1)} copy(bf16[32,128]{1,0:T(8,128)(2,1)} %mix_out_and_unit.1) | data formatting | bytes 16384
  (25 shorter events, 0.2 us)
Async XLA Ops:
  0.0 50.5 %copy-start = (f32[4,16,64,128]{3,2,1,0:T(8,128)S(1)}, f32[4,16,64,128]{3,2,1,0:T(8,128)}, u32[]{:S(2)}) copy-start(f32[4,16,64,128]{3,2,1,0:T(8,128)} %param.48) | copy-start | bytes 6291460
  0.0 44.7 %copy-start.7 = (f32[4,512]{1,0:T(4,128)S(1)}, f32[4,512]{1,0:T(4,128)}, u32[]{:S(2)}) copy-start(f32[4,512]{1,0:T(4,128)} %param.42) | copy-start | bytes 24580
  0.0 44.7 %copy-start.8 = (f32[4,512]{1,0:T(4,128)S(1)}, f32[4,512]{1,0:T(4,128)}, u32[]{:S(2)}) copy-start(f32[4,512]{1,0:T(4,128)} %param.43) | copy-start | bytes 24580
  0.0 44.7 %copy-start.9 = (bf16[4,3,512]{2,0,1:T(4,128)(2,1)S(1)}, bf16[4,3,512]{2,0,1:T(4,128)(2,1)}, u32[]{:S(2)}) copy-start(bf16[4,3,512]{2,0,1:T(4,128)(2,1)} %param.45) | copy-start | bytes 36868
  0.0 44.7 %copy-start.10 = (bf16[4,3,512]{2,0,1:T(4,128)(2,1)S(1)}, bf16[4,3,512]{2,0,1:T(4,128)(2,1)}, u32[]{:S(2)}) copy-start(bf16[4,3,512]{2,0,1:T(4,128)(2,1)} %param.46) | copy-start | bytes 36868
  0.0 45.7 %copy-start.12 = (s32[4]{0:T(128)S(1)}, s32[4]{0:T(128)}, u32[]{:S(2)}) copy-start(s32[4]{0:T(128)} %param.53) | copy-start | bytes 52
  0.0 45.8 %copy-start.4 = (f32[4,128,16]{1,2,0:T(8,128)S(1)}, f32[4,128,16]{1,2,0:T(8,128)}, u32[]{:S(2)}) copy-start(f32[4,128,16]{1,2,0:T(8,128)} %param.52) | copy-start | bytes 98308
  0.0 46.9 %copy-start.13 = (f32[16]{0:T(128)S(1)}, f32[16]{0:T(128)}, u32[]{:S(2)}) copy-start(f32[16]{0:T(128)} %param.47) | copy-start | bytes 196
  0.1 47.0 %copy-start.1 = (bf16[4,128,512]{2,1,0:T(8,128)(2,1)S(1)}, bf16[4,128,512]{2,1,0:T(8,128)(2,1)}, u32[]{:S(2)}) copy-start(bf16[4,128,512]{2,1,0:T(8,128)(2,1)} %param.49) | copy-start | bytes 1572868
  44.7 3.1 %copy-start.3 = (f32[4,128,16]{1,2,0:T(8,128)S(1)}, f32[4,128,16]{1,2,0:T(8,128)}, u32[]{:S(2)}) copy-start(f32[4,128,16]{1,2,0:T(8,128)} %param.51) | copy-start | bytes 98308
  49.8 4.1 %copy-start.5 = (f32[4,1024]{1,0:T(4,128)S(1)}, f32[4,1024]{1,0:T(4,128)}, u32[]{:S(2)}) copy-start(f32[4,1024]{1,0:T(4,128)} %param.41) | copy-start | bytes 49156
  49.8 4.1 %copy-start.6 = (bf16[4,3,1024]{2,0,1:T(4,128)(2,1)S(1)}, bf16[4,3,1024]{2,0,1:T(4,128)(2,1)}, u32[]{:S(2)}) copy-start(bf16[4,3,1024]{2,0,1:T(4,128)(2,1)} %param.44) | copy-start | bytes 73732
  49.8 4.1 %copy-start.2 = (f32[4,3200]{1,0:T(4,128)S(1)}, f32[4,3200]{1,0:T(4,128)}, u32[]{:S(2)}) copy-start(f32[4,3200]{1,0:T(4,128)} %get-tuple-element.8) | copy-start | bytes 153604
  49.8 4.5 %copy-start.11 = (f32[1024]{0:T(1024)S(1)}, f32[1024]{0:T(1024)}, u32[]{:S(2)}) copy-start(f32[1024]{0:T(1024)} %param.54) | copy-start | bytes 12292

commit v2 on v0

--- a/solution.py
+++ b/solution.py
@@ -1,7 +1,16 @@
+import functools
+import math
+
 import jax
 import jax.numpy as jnp
 from jax import lax
+from jax.experimental import pallas as pl
+from jax.experimental.pallas import tpu as pltpu
 from jax.sharding import PartitionSpec as P
+
+MESH_ID = pl.DeviceIdType.MESH
+LANES = 128
+SHORT = jnp.bfloat16
 
 D = 2048
 GROUPS = 8
@@ -9,6 +18,605 @@
 
 
 EPSILON = 1e-06
+
+
+class Plan:
+    def __init__(self, kv, rows, own_rows, width, hidden, seqs):
+        inner = max(i for i in range(1, math.isqrt(kv) + 1) if kv % i == 0)
+        self.kv, self.inner, self.outer = kv, inner, kv // inner
+        self.rows, self.own_rows, self.width = rows, own_rows, width
+        self.model = width * kv
+        self.group = rows // inner
+        self.seqs = seqs
+        tiles = hidden // LANES
+        wide = -(-tiles // self.outer)
+        self.starts = [c * (tiles - wide) // max(self.outer - 1, 1) * LANES for c in range(self.outer)]
+        self.tiles, self.wide_tiles = tiles, wide
+        self.wide = wide * LANES
+        ends = self.starts[1:] + [tiles * LANES]
+        self.used = [e - s for s, e in zip(self.starts, ends)]
+
+    def start(self, c):
+        first = (c * (self.tiles - self.wide_tiles)) // max(self.outer - 1, 1)
+        return pl.multiple_of(first * LANES, LANES)
+
+
+def place(plan):
+    k = lax.axis_index("kv")
+    return lax.div(k, plan.inner), lax.rem(k, plan.inner), lax.axis_index("tp")
+
+
+def greet(plan, z, p, t):
+    barrier = pltpu.get_barrier_semaphore()
+    for d in range(1, plan.inner):
+        pl.semaphore_signal(barrier, inc=1, device_id=plane_peer(plan, z, p, t, d), device_id_type=MESH_ID)
+    for d in range(1, plan.outer):
+        pl.semaphore_signal(barrier, inc=1, device_id=line_peer(plan, z, p, t, d), device_id_type=MESH_ID)
+    pl.semaphore_signal(barrier, inc=1, device_id=(z * plan.inner + p, 1 - t), device_id_type=MESH_ID)
+    pl.semaphore_wait(barrier, plan.inner + plan.outer - 1)
+
+
+def plane_peer(plan, z, p, t, d):
+    return (z * plan.inner + lax.rem(p + d, plan.inner), t)
+
+
+def line_peer(plan, z, p, t, d):
+    return (lax.rem(z + d, plan.outer) * plan.inner + p, t)
+
+
+def remote(src, dst, sems, index, device):
+    return pltpu.make_async_remote_copy(
+        src_ref=src,
+        dst_ref=dst,
+        send_sem=sems.at[(0,) + index],
+        recv_sem=sems.at[(1,) + index],
+        device_id=device,
+        device_id_type=MESH_ID,
+    )
+
+
+def silu(a):
+    return a / (1.0 + jnp.exp(-a))
+
+
+def unit_scratch(plan):
+    span = 2 * plan.wide + LANES
+    i, o, g = plan.inner, plan.outer, plan.group
+    return [
+        pltpu.VMEM((i, o, g, span), jnp.bfloat16),
+        pltpu.VMEM((i, o, g, span), jnp.bfloat16),
+        pltpu.VMEM((o, g, span), jnp.bfloat16),
+        pltpu.VMEM((o, g, span), jnp.bfloat16),
+        pltpu.VMEM((o, i, g, plan.wide), jnp.bfloat16),
+        pltpu.SemaphoreType.DMA((2, i, o)),
+        pltpu.SemaphoreType.DMA((2, o)),
+        pltpu.SemaphoreType.DMA((2, o)),
+        pltpu.SemaphoreType.DMA((2, i, o)),
+    ]
+
+
+def unit_product(plan, x, gain, gate_ref, lift_ref, drop_ref, scratch):
+    out_buf, in_buf, line_out, line_in, hid, plane_sem, line_sem, hz_sem, hp_sem = scratch
+    z, p, t = place(plan)
+    inner, outer, group, wide = plan.inner, plan.outer, plan.group, plan.wide
+    values = x.astype(jnp.float32)
+    squares = jnp.sum(values * values, axis=1, keepdims=True)
+    squares = jnp.broadcast_to(squares, (plan.rows, LANES)).astype(jnp.bfloat16)
+    scaled = (values * gain).astype(jnp.bfloat16)
+    sends = []
+    plane = []
+    for n in range(outer):
+        c = lax.rem(z + 1 + n, outer)
+        columns = pl.ds(plan.start(c), wide)
+        gate = jnp.dot(scaled, gate_ref[:, columns], preferred_element_type=jnp.float32).astype(jnp.bfloat16)
+        lift = jnp.dot(scaled, lift_ref[:, columns], preferred_element_type=jnp.float32).astype(jnp.bfloat16)
+        for q in range(inner):
+            rows = slice(q * group, (q + 1) * group)
+            out_buf[q, n, :, 0:wide] = gate[rows]
+            out_buf[q, n, :, wide : 2 * wide] = lift[rows]
+            out_buf[q, n, :, 2 * wide :] = squares[rows]
+        copies = []
+        for d in range(1, inner):
+            copy = remote(
+                out_buf.at[lax.rem(p + d, inner), n],
+                in_buf.at[d, n],
+                plane_sem,
+                (d, n),
+                plane_peer(plan, z, p, t, d),
+            )
+            copy.start()
+            copies.append(copy)
+        plane.append(copies)
+        sends.extend(copies)
+    line = []
+    for n in range(outer):
+        total = out_buf[p, n].astype(jnp.float32)
+        for d in range(1, inner):
+            plane[n][d - 1].wait_recv()
+            total = total + in_buf[d, n].astype(jnp.float32)
+        if n < outer - 1:
+            line_out[n] = total.astype(jnp.bfloat16)
+            copy = remote(line_out.at[n], line_in.at[n], line_sem, (n,), line_peer(plan, z, p, t, n + 1))
+            copy.start()
+            line.append(copy)
+    sends.extend(line)
+    for n in range(outer - 1):
+        line[n].wait_recv()
+        total = total + line_in[n].astype(jnp.float32)
+    scale = lax.rsqrt(total[:, 2 * wide :] / plan.model + EPSILON)[:, 0:1]
+    hidden = silu(total[:, 0:wide] * scale) * (total[:, wide : 2 * wide] * scale)
+    hid[z, p] = hidden.astype(jnp.bfloat16)
+    line = []
+    for d in range(1, outer):
+        copy = remote(hid.at[z, p], hid.at[z, p], hz_sem, (d,), line_peer(plan, z, p, t, d))
+        copy.start()
+        line.append(copy)
+    sends.extend(line)
+
+    def from_line(d):
+        source = lax.rem(z + outer - d, outer)
+        return remote(hid.at[source, p], hid.at[source, p], hz_sem, (d,), line_peer(plan, z, p, t, d))
+
+    for n in range(outer):
+        source = lax.rem(z + outer - n, outer)
+        if n > 0:
+            from_line(n).wait_recv()
+        for d in range(1, inner):
+            copy = remote(hid.at[source, p], hid.at[source, p], hp_sem, (d, n), plane_peer(plan, z, p, t, d))
+            copy.start()
+            sends.append(copy)
+    for n in range(outer):
+        source = lax.rem(z + outer - n, outer)
+        for d in range(1, inner):
+            sender = lax.rem(p + inner - d, inner)
+            remote(
+                hid.at[source, sender], hid.at[source, sender], hp_sem, (d, n), plane_peer(plan, z, p, t, d)
+            ).wait_recv()
+    total = jnp.zeros((plan.rows, plan.width), jnp.float32)
+    for c in range(outer):
+        first, used = plan.starts[c], plan.used[c]
+        lhs = hid[c, :, :, 0:used].reshape(plan.rows, used)
+        total = total + jnp.dot(lhs, drop_ref[first : first + used, :], preferred_element_type=jnp.float32)
+    return total.astype(jnp.bfloat16), sends
+
+
+def swap_whole(plan, mine, pair, sem):
+    z, p, t = place(plan)
+    pair[0] = mine
+    copy = remote(pair.at[0], pair.at[1], sem, (0,), (z * plan.inner + p, 1 - t))
+    copy.start()
+    copy.wait()
+    return mine.astype(jnp.float32) + pair[1].astype(jnp.float32)
+
+
+def block_mix(
+    plan,
+    raw,
+    lengths_ref,
+    vtap_ref,
+    ktap_ref,
+    qtap_ref,
+    vpast_ref,
+    kpast_ref,
+    qpast_ref,
+    rate_ref,
+    head_gain_ref,
+    state_high,
+    state_low,
+    keys_ref,
+    values_ref,
+    steps_ref,
+    decay_ref,
+    prepared,
+):
+    t = lax.axis_index("tp")
+    heads, block_len = decay_ref.shape[1], decay_ref.shape[2]
+    head_dim, states = state_high.shape[1] // heads, state_high.shape[2]
+    groups = keys_ref.shape[2] // states
+    per_group = heads // groups
+    channels = heads * head_dim
+    key_raw, query_raw, step_rows, value_raw, gate_rows = raw
+
+    def convolve(past_ref, tap_ref, newest):
+        last = tap_ref.shape[0] - 1
+        total = tap_ref[last : last + 1, :] * newest
+        for k in range(last):
+            total = total + past_ref[k].astype(jnp.float32) * tap_ref[k : k + 1, :]
+        return silu(total)
+
+    new_value = convolve(vpast_ref, vtap_ref, value_raw)
+    new_key = convolve(kpast_ref, ktap_ref, key_raw)
+    new_query = convolve(qpast_ref, qtap_ref, query_raw)
+    gate = silu(gate_rows)
+
+    def iota(shape, dim):
+        return lax.broadcasted_iota(jnp.int32, shape, dim)
+
+    own_group = lax.div(iota((heads, groups * states), 0), per_group) == lax.div(
+        iota((heads, groups * states), 1), states
+    )
+    own_head = iota((heads, channels), 0) == lax.div(iota((heads, channels), 1), head_dim)
+    own_step = iota((heads, LANES), 1) == iota((heads, LANES), 0) + t * heads
+    own_rate = iota((heads, heads), 0) == iota((heads, heads), 1)
+    rate = jnp.sum(jnp.where(own_rate, rate_ref[...], 0.0), axis=1, keepdims=True)
+    rows = []
+    for s in range(plan.seqs):
+        tail, total, live = prepared[s]
+        step_raw = jnp.sum(jnp.where(own_step, step_rows[s : s + 1], 0.0), axis=1, keepdims=True)
+        step_size = jnp.maximum(step_raw, 0.0) + jnp.log1p(jnp.exp(-jnp.abs(step_raw)))
+        new_decay = -rate * step_size
+        query_spread = jnp.where(own_group, new_query[s : s + 1], 0.0)
+        key_spread = jnp.where(own_group, new_key[s : s + 1], 0.0)
+        scores = lax.dot_general(
+            query_spread.astype(jnp.bfloat16),
+            keys_ref[s],
+            (((1,), (1,)), ((), ())),
+            preferred_element_type=jnp.float32,
+        )
+        weights = jnp.where(live, jnp.exp(tail + new_decay) * steps_ref[s] * scores, 0.0).astype(jnp.bfloat16)
+        from_block = jnp.dot(weights, values_ref[s], preferred_element_type=jnp.float32)
+        query_heads = query_spread[:, 0:states]
+        for g in range(1, groups):
+            query_heads = query_heads + query_spread[:, g * states : (g + 1) * states]
+        high = query_heads.astype(jnp.bfloat16)
+        low = (query_heads - high.astype(jnp.float32)).astype(jnp.bfloat16)
+
+        def contract(rows_in, block):
+            return lax.dot_general(
+                rows_in, block, (((1,), (1,)), ((), ())), preferred_element_type=jnp.float32
+            )
+
+        both = contract(jnp.concatenate([high, low], axis=0), state_high[s])
+        from_state = both[0:heads] + both[heads:] + contract(high, state_low[s])
+        self_score = jnp.sum(query_spread * key_spread, axis=1, keepdims=True)
+        mixed = jnp.exp(total + new_decay) * from_state + from_block
+        mixed = mixed + (step_size * self_score) * new_value[s : s + 1]
+        mixed = jnp.where(own_head, mixed * gate[s : s + 1], 0.0)
+        mean = jnp.sum(mixed * mixed, axis=1, keepdims=True) / head_dim
+        mixed = mixed * lax.rsqrt(mean + EPSILON)
+        rows.append(jnp.sum(mixed, axis=0, keepdims=True) * head_gain_ref[...])
+    return rows
+
+
+def prepare_block(plan, lengths_ref, decay_ref):
+    heads, block_len = decay_ref.shape[1], decay_ref.shape[2]
+    after = lax.broadcasted_iota(jnp.int32, (block_len, block_len), 0) > lax.broadcasted_iota(
+        jnp.int32, (block_len, block_len), 1
+    )
+    after = jnp.where(after, 1.0, 0.0)
+    position = lax.broadcasted_iota(jnp.int32, (heads, block_len), 1)
+    out = []
+    for s in range(plan.seqs):
+        live = position < lengths_ref[s] - 1
+        masked = jnp.where(live, decay_ref[s], 0.0)
+        tail = jnp.dot(masked, after, precision=lax.Precision.HIGHEST, preferred_element_type=jnp.float32)
+        out.append((tail, jnp.sum(masked, axis=1, keepdims=True), live))
+    return out
+
+
+SMALL = 15
+LOADED = 15
+
+
+def layer_kernel(plan, *refs):
+    (x_ref, gain_ref, mix_gain_ref, step_ref, lengths_ref, vtap_ref, ktap_ref, qtap_ref) = refs[:8]
+    (vpast_ref, kpast_ref, qpast_ref, rate_ref, head_gain_ref, gain_after_ref, decay_ref) = refs[8:SMALL]
+    stored = refs[SMALL : SMALL + LOADED]
+    out_ref = refs[SMALL + LOADED]
+    rest = refs[SMALL + LOADED + 1 :]
+    held, rest = rest[:LOADED], rest[LOADED:]
+    load_sem, rest = rest[0], rest[1:]
+    (
+        gathered,
+        gather_sem,
+        pair_one,
+        pair_sem_one,
+        mix_out,
+        mix_in,
+        mline_out,
+        mline_in,
+        mplane_sem,
+        mline_sem,
+        mixed,
+        stacked,
+        pair_two,
+        pair_sem_two,
+        final_in,
+        final_out,
+        section_buf,
+        mz_sem,
+        mp_sem,
+        final_sem,
+        state_high,
+        state_low,
+    ) = rest[:22]
+    unit = len(unit_scratch(plan))
+    scratch_one, scratch_two = rest[22 : 22 + unit], rest[22 + unit :]
+    loads = [pltpu.make_async_copy(stored[n], held[n], load_sem.at[n]) for n in range(LOADED)]
+    for load in loads:
+        load.start()
+    (gate_ref, lift_ref, drop_ref, value_ref, mgate_ref, key_ref, query_ref) = held[:7]
+    (keys_ref, values_ref, steps_ref, state_ref, out_proj_ref, gate2_ref, lift2_ref, drop2_ref) = held[7:]
+
+    z, p, t = place(plan)
+    inner, outer, group, seqs = plan.inner, plan.outer, plan.group, plan.seqs
+    greet(plan, z, p, t)
+    first_copy = remote(x_ref, gathered.at[t], gather_sem, (0,), (z * inner + p, 1 - t))
+    first_copy.start()
+    gathered[t] = x_ref[...]
+    prepared = prepare_block(plan, lengths_ref, decay_ref)
+    for load in loads[:3]:
+        load.wait()
+    remote(x_ref, gathered.at[1 - t], gather_sem, (0,), (z * inner + p, 1 - t)).wait_recv()
+    x = gathered[...].reshape(plan.rows, plan.width)
+    product, sends = unit_product(plan, x, gain_ref[...], gate_ref, lift_ref, drop_ref, scratch_one)
+    sends.append(first_copy)
+    unit_sum = swap_whole(plan, product, pair_one, pair_sem_one)
+    section = (x.astype(jnp.float32) + 0.5 * unit_sum).astype(jnp.bfloat16)
+    at = lax.broadcasted_iota(jnp.int32, (plan.rows, plan.rows), 0)
+    of = lax.broadcasted_iota(jnp.int32, (plan.rows, plan.rows), 1)
+    own_inner = lax.div(at, outer * seqs)
+    left = at - own_inner * (outer * seqs)
+    own_outer = lax.div(left, seqs)
+    wanted = (own_outer * inner + own_inner) * seqs + (left - own_outer * seqs)
+    moving = jnp.where(of == wanted, 1.0, 0.0).astype(jnp.bfloat16)
+    values = jnp.dot(moving, section, preferred_element_type=jnp.float32)
+    squares = jnp.sum(values * values, axis=1, keepdims=True)
+    scaled = (values * mix_gain_ref[...]).astype(jnp.bfloat16)
+    steps = step_ref.shape[0]
+    row = lax.broadcasted_iota(jnp.int32, (LANES, steps), 0)
+    lane = lax.broadcasted_iota(jnp.int32, (LANES, steps), 1)
+    spread = jnp.where(row == lane, 1.0, 0.0).astype(jnp.bfloat16)
+    step_wide = jnp.dot(spread, step_ref[...], preferred_element_type=jnp.float32).astype(jnp.bfloat16)
+    lanes = lax.broadcasted_iota(jnp.int32, (plan.rows, LANES), 1)
+    last = lax.dot_general(scaled, step_wide, (((1,), (1,)), ((), ())), preferred_element_type=jnp.float32)
+    last = jnp.where(lanes == LANES - 1, squares, last).astype(jnp.bfloat16)
+    for load in loads[3:7]:
+        load.wait()
+    chunks, first = [], 0
+    plane = []
+    for n, parts in enumerate(((key_ref, query_ref), (value_ref,), (mgate_ref,))):
+        low = first
+        pieces = [jnp.dot(scaled, ref[...], preferred_element_type=jnp.float32).astype(jnp.bfloat16) for ref in parts]
+        if n == 0:
+            pieces.append(last)
+        for piece in pieces:
+            size = piece.shape[1]
+            for q in range(inner):
+                mix_out[q, :, first : first + size] = piece[q * group : (q + 1) * group]
+            first = first + size
+        columns = slice(low, first)
+        chunks.append(columns)
+        copies = []
+        for d in range(1, inner):
+            copy = remote(
+                mix_out.at[lax.rem(p + d, inner), :, columns],
+                mix_in.at[d, :, columns],
+                mplane_sem,
+                (d, n),
+                plane_peer(plan, z, p, t, d),
+            )
+            copy.start()
+            copies.append(copy)
+        plane.append(copies)
+        sends.extend(copies)
+    for load in loads[7:]:
+        load.wait()
+    for s in range(seqs):
+        state = state_ref[s]
+        high = state.astype(jnp.bfloat16)
+        state_high[s] = high
+        state_low[s] = (state - high.astype(jnp.float32)).astype(jnp.bfloat16)
+    line = []
+    for n, columns in enumerate(chunks):
+        total = mix_out[p, :, columns].astype(jnp.float32)
+        for d in range(1, inner):
+            plane[n][d - 1].wait_recv()
+            total = total + mix_in[d, :, columns].astype(jnp.float32)
+        for o in range(outer):
+            mline_out[o, :, columns] = total[o * seqs : (o + 1) * seqs].astype(mline_out.dtype)
+        copies = []
+        for d in range(1, outer):
+            copy = remote(
+                mline_out.at[lax.rem(z + d, outer), :, columns],
+                mline_in.at[d, :, columns],
+                mline_sem,
+                (d, n),
+                line_peer(plan, z, p, t, d),
+            )
+            copy.start()
+            copies.append(copy)
+        line.append(copies)
+        sends.extend(copies)
+    totals = []
+    for n, columns in enumerate(chunks):
+        total = mline_out[z, :, columns].astype(jnp.float32)
+        for d in range(1, outer):
+            line[n][d - 1].wait_recv()
+            total = total + mline_in[d, :, columns].astype(jnp.float32)
+        totals.append(total)
+    scale = lax.rsqrt(totals[0][:, -1:] / plan.model + EPSILON)
+    totals = [total * scale for total in totals]
+    keys_end, query_end = key_ref.shape[1], key_ref.shape[1] + query_ref.shape[1]
+    raw = (
+        totals[0][:, :keys_end],
+        totals[0][:, keys_end:query_end],
+        totals[0][:, query_end:],
+        totals[1],
+        totals[2],
+    )
+    rows = block_mix(
+        plan,
+        raw,
+        lengths_ref,
+        vtap_ref,
+        ktap_ref,
+        qtap_ref,
+        vpast_ref,
+        kpast_ref,
+        qpast_ref,
+        rate_ref,
+        head_gain_ref,
+        state_high,
+        state_low,
+        keys_ref,
+        values_ref,
+        steps_ref,
+        decay_ref,
+        prepared,
+    )
+    mixed[z, p] = jnp.concatenate(rows, axis=0).astype(mixed.dtype)
+    own = mixed.at[z, p]
+    for d in range(1, outer):
+        copy = remote(own, own, mz_sem, (d,), line_peer(plan, z, p, t, d))
+        copy.start()
+        sends.append(copy)
+    for n in range(outer):
+        source = lax.rem(z + outer - n, outer)
+        block = mixed.at[source, p]
+        if n > 0:
+            remote(block, block, mz_sem, (n,), line_peer(plan, z, p, t, n)).wait_recv()
+        for d in range(1, inner):
+            copy = remote(block, block, mp_sem, (d, n), plane_peer(plan, z, p, t, d))
+            copy.start()
+            sends.append(copy)
+    for n in range(outer):
+        source = lax.rem(z + outer - n, outer)
+        for d in range(1, inner):
+            block = mixed.at[source, lax.rem(p + inner - d, inner)]
+            remote(block, block, mp_sem, (d, n), plane_peer(plan, z, p, t, d)).wait_recv()
+    for o in range(outer):
+        for i in range(inner):
+            first = (o * inner + i) * seqs
+            stacked[first : first + seqs, :] = mixed[o, i].astype(jnp.float32)
+    product = jnp.dot(
+        stacked[...].astype(jnp.bfloat16), out_proj_ref[...], preferred_element_type=jnp.float32
+    ).astype(jnp.bfloat16)
+    branch = swap_whole(plan, product, pair_two, pair_sem_two)
+    x = (section.astype(jnp.float32) + branch).astype(jnp.bfloat16)
+    section_buf[...] = x.reshape(section_buf.shape)
+    product, more = unit_product(plan, x, gain_after_ref[...], gate2_ref, lift2_ref, drop2_ref, scratch_two)
+    final_out[...] = product.reshape(final_out.shape)
+    copy = remote(final_out.at[1 - t], final_in, final_sem, (0,), (z * inner + p, 1 - t))
+    copy.start()
+    copy.wait()
+    unit_sum = final_out[t].astype(jnp.float32) + final_in[...].astype(jnp.float32)
+    out_ref[...] = (section_buf[t].astype(jnp.float32) + 0.5 * unit_sum).astype(jnp.bfloat16)
+    for copy in sends + more:
+        copy.wait_send()
+
+
+def on_device_fast(
+    hidden_in,
+    gain_before,
+    gate_before,
+    lift_before,
+    drop_before,
+    mixer_gain,
+    value_proj,
+    gate_proj,
+    key_proj,
+    query_proj,
+    step_proj,
+    value_taps,
+    key_taps,
+    query_taps,
+    value_past,
+    key_past,
+    query_past,
+    decay_rate,
+    block_state,
+    block_keys,
+    block_values,
+    block_steps,
+    block_decay,
+    lengths,
+    head_gain,
+    out_proj,
+    gain_after,
+    gate_after,
+    lift_after,
+    drop_after,
+):
+    kv, tp = lax.axis_size("kv"), lax.axis_size("tp")
+    own_rows, width = hidden_in.shape
+    rows, hidden, seqs = own_rows * tp, gate_before.shape[1], lengths.shape[0]
+    plan = Plan(kv, rows, own_rows, width, hidden, seqs)
+    channels = value_proj.shape[1]
+    span = channels + gate_proj.shape[1] + key_proj.shape[1] + query_proj.shape[1] + LANES
+    i, o, g, s = plan.inner, plan.outer, plan.group, seqs
+    vmem = pl.BlockSpec(memory_space=pltpu.VMEM)
+    smem = pl.BlockSpec(memory_space=pltpu.SMEM)
+    anywhere = pl.BlockSpec(memory_space=pl.ANY)
+    small = (
+        hidden_in,
+        gain_before[None],
+        mixer_gain[None],
+        step_proj.T,
+        lengths,
+        value_taps,
+        key_taps,
+        query_taps,
+        value_past.transpose(1, 0, 2),
+        key_past.transpose(1, 0, 2),
+        query_past.transpose(1, 0, 2),
+        decay_rate[None],
+        head_gain[None],
+        gain_after[None],
+        block_decay.transpose(0, 2, 1),
+    )
+    loaded = (
+        gate_before,
+        lift_before,
+        drop_before,
+        value_proj,
+        gate_proj,
+        key_proj,
+        query_proj,
+        block_keys,
+        block_values,
+        block_steps.transpose(0, 2, 1),
+        block_state.reshape(seqs, channels, block_state.shape[3]),
+        out_proj,
+        gate_after,
+        lift_after,
+        drop_after,
+    )
+    dma, half, full = pltpu.SemaphoreType.DMA, jnp.bfloat16, jnp.float32
+    scratch = [pltpu.VMEM(array.shape, array.dtype) for array in loaded] + [
+        dma((len(loaded),)),
+        pltpu.VMEM((2, own_rows, width), half),
+        dma((2, 1)),
+        pltpu.VMEM((2, rows, width), half),
+        dma((2, 1)),
+        pltpu.VMEM((i, g, span), half),
+        pltpu.VMEM((i, g, span), half),
+        pltpu.VMEM((o, s, span), SHORT),
+        pltpu.VMEM((o, s, span), SHORT),
+        dma((2, i, 3)),
+        dma((2, o, 3)),
+        pltpu.VMEM((o, i, s, channels), SHORT),
+        pltpu.VMEM((rows, channels), full),
+        pltpu.VMEM((2, rows, width), half),
+        dma((2, 1)),
+        pltpu.VMEM((own_rows, width), half),
+        pltpu.VMEM((2, own_rows, width), half),
+        pltpu.VMEM((2, own_rows, width), half),
+        dma((2, o)),
+        dma((2, i, o)),
+        dma((2, 1)),
+        pltpu.VMEM((s, channels, block_state.shape[3]), half),
+        pltpu.VMEM((s, channels, block_state.shape[3]), half),
+    ]
+    return pl.pallas_call(
+        functools.partial(layer_kernel, plan),
+        out_shape=jax.ShapeDtypeStruct((own_rows, width), jnp.bfloat16),
+        in_specs=[smem if array is lengths else vmem for array in small] + [anywhere] * len(loaded),
+        out_specs=vmem,
+        scratch_shapes=scratch + unit_scratch(plan) + unit_scratch(plan),
+        compiler_params=pltpu.CompilerParams(collective_id=0, has_side_effects=True),
+        name="layer",
+    )(*small, *loaded)
 
 
 def gather_rows(rows_in, gain_vec):
@@ -231,9 +839,69 @@
     ).astype(jnp.bfloat16)
 
 
+def fits(
+    hidden_in,
+    gain_before,
+    gate_before,
+    lift_before,
+    drop_before,
+    mixer_gain,
+    value_proj,
+    gate_proj,
+    key_proj,
+    query_proj,
+    step_proj,
+    value_taps,
+    key_taps,
+    query_taps,
+    value_past,
+    key_past,
+    query_past,
+    decay_rate,
+    block_state,
+    block_keys,
+    block_values,
+    block_steps,
+    block_decay,
+    lengths,
+    head_gain,
+    out_proj,
+    gain_after,
+    gate_after,
+    lift_after,
+    drop_after,
+):
+    kv, tp = lax.axis_size("kv"), lax.axis_size("tp")
+    own_rows, width = hidden_in.shape
+    inner = max(i for i in range(1, math.isqrt(kv) + 1) if kv % i == 0)
+    aligned = (
+        gate_before.shape[1],
+        width,
+        value_proj.shape[1],
+        gate_proj.shape[1],
+        key_proj.shape[1],
+        query_proj.shape[1],
+    )
+    return (
+        tp == 2
+        and inner > 1
+        and all(size % LANES == 0 for size in aligned)
+        and own_rows % 16 == 0
+        and own_rows * tp % (16 * inner) == 0
+        and lengths.shape[0] in (4, 8)
+        and lengths.shape[0] * kv == own_rows * tp
+        and step_proj.shape[1] < LANES
+        and gate_before.shape[1] // LANES >= 2 * (kv // inner)
+    )
+
+
+def choose(*args):
+    return on_device_fast(*args) if fits(*args) else on_device(*args)
+
+
 def solution(mesh):
     return jax.shard_map(
-        on_device,
+        choose,
         mesh=mesh,
         in_specs=(
             P("tp", "kv"),

time: 465 us -> 79.5 us (0.17)
  blocking collectives: 211 us -> 0 us
  waiting for transfers between devices: 199 us -> 0 us
  Pallas kernels: 0 us -> 77.9 us
  matrix products: 24 us -> 0 us
  between operations: 14.5 us -> 0.01 us
  other arithmetic: 7.7 us -> 0 us
  local copies, waits for them, and re-layouts: 8.42 us -> 1.3 us
    psum x3 -> x0, blocking collectives: 163 us -> none  [the longest x2 85.9 us: half_mlp(): totals = lax.psum(squares, 'kv')]
    psum x2 -> x0, waiting for transfers between devices: 150 us -> none  [half_mlp(): gate_sum, lift_sum = lax.psum((gate_part, lift_part), 'kv')]
    pallas_call x0 -> x1, Pallas kernels: none -> 77.9 us  [on_device_fast(): pl.pallas_call(functools.partial(layer_kernel, plan), out_shape=jax.Shape...]
    all_gather x4 -> x0, blocking collectives: 47.5 us -> none  [the longest x1 41.6 us: mixer(): lax.all_gather(mixed_rows, 'kv', axis=0, tiled=True)]
    unnamed x7 -> x0, waiting for transfers between devices: 31 us -> none
    dot_general x15 -> x0, matrix products: 24 us -> none  [the longest x2 5.19 us: half_mlp(): jnp.dot(hidden, drop_weight, preferred_element_type=jnp.float32)]
    reduce_scatter x3 -> x0, waiting for transfers between devices: 17.7 us -> none  [finish(): lax.psum_scatter(partial_value.astype(jnp.float32).astype(jnp.bfloat16),...]
    unnamed x63 -> x1, local copies, waits for them, and re-layouts: 6.1 us -> 1.3 us
  transfers between devices with their start and end apart: 6 -> 0, of which waited for: 6 -> 0; matrix products, arithmetic and copies ran while one was open for 1% -> 0% of each run, Pallas kernels for 0% -> 0%
where the time goes in v2:
time: 79.5 us; the launch traced here: 79.2 us
  Pallas kernels  77.9 us (98%)
  local copies, waits for them, and re-layouts  1.3 us (2%)
    pallas_call x1, Pallas kernels, on_device_fast(): pl.pallas_call(functools.partial(layer_kernel, plan), out_shape=jax.Shape...  77.9 us

profile of v2, /device:TPU:0, one launch (start us, length us, event | category | flops | bytes accessed | tf_op | source)
XLA Modules:
  0.0 79.2 jit_solution(2914125296095609687)
XLA Ops:
  0.0 77.9 %layer.1 = bf16[32,128]{1,0:T(8,128)(2,1)} custom-call(bf16[32,128]{1,0:T(8,128)(2,1)} %refs_0_.1, f32[1,128]{1,0:T(1,128)} %bitcast.20, f32[1,128]{1,0:T(1,128)} %bitcast.21, bf16[32,128]{1,0:T(8,128)(2,1)} %bitcast.18, s32[4]{0:T(128)} %refs_4_.1, f32[4,1024]{1,0:T(4,128)} %refs_5_.1, f32[4,512]{1,0:T(4,128)} %refs_6_.1, f32[4,512]{1,0:T(4,128)} %refs_7_.1, ...), custom_call_target="tpu_custom_call" | custom-call | tf_op jit(solution)/shard_map/layer/pallas_call | solution.py:611
  77.9 1.3 %copy.32 = bf16[32,128]{1,0:T(8,128)(2,1)} copy(bf16[32,128]{1,0:T(8,128)(2,1)} %layer.1) | data formatting | bytes 16384
